TPU v7x, 32 devices: a whole 2x2x4 slice. The times are simulated.
32 devices in a mesh: sp: 8 (over z, x), dp: 4 (over y, core).
Axes of the slice: x: 2, y: 2, z: 4, core: 2. Of those that a mesh axis runs over, the one named last changes fastest.
Arguments:
- queries: bfloat16 [4, 1024, 2048], P('dp', 'sp'), may hold values from -12 to 12
- key_rows: bfloat16 [4, 1024, 2048], P('dp', 'sp'), may hold values from -12 to 12
- value_rows: bfloat16 [4, 1024, 2048], P('dp', 'sp'), may hold values from -6 to 6
- lambdas: float32 [16], P('sp'), may hold values from 0.3 to 0.8
- head_gain: float32 [128], replicated, may hold values from 0.1 to 1.9
- out_weight: bfloat16 [2048, 2048], replicated, may hold values from -0.125 to 0.125
- residual: bfloat16 [4, 1024, 2048], P('dp', 'sp'), may hold values from -6 to 6
- mixer_gain: float32 [2048], replicated, may hold values from 0.1 to 1.9
- channel_gain: float32 [2048], replicated, may hold values from 0.1 to 1.9
- expert_gain: float32 [2048], replicated, may hold values from 0.1 to 1.9
- routes: int32 [4, 1024, 2], P('dp', 'sp'), may hold values from 0 to 7, all different within a row; in each aligned block of 128 rows (0 to 127, 128 to 255, ..., all dimensions but the last counted through in order) at most 48 rows name the same one
- route_logits: float32 [4, 1024, 2], P('dp', 'sp'), may hold values from -5 to 5
- gate_weight: bfloat16 [8, 2048, 4096], P('sp', None, 'dp'), may hold values from -0.125 to 0.125
- up_weight: bfloat16 [8, 2048, 4096], P('sp', None, 'dp'), may hold values from -0.125 to 0.125
- down_weight: bfloat16 [8, 4096, 2048], P('sp', 'dp'), may hold values from -0.09375 to 0.09375
Outputs:
- updated: bfloat16 [4, 1024, 2048], P('dp', 'sp')
Inputs may be any that keep to these rules, and one draw needn't show every extreme that they name: `routes`: among the rows of one device no expert is named by more than 48 rows; in some of these blocks one expert is named by exactly 48.
All inputs are finite; a program needn't handle non-finite values.
Results may differ from a plain program's by a relative error of at most 0.014.
Values may be sent and summed in bfloat16 or wider, within the bound.
A program may use at most 128 MiB of HBM per device.

v0:
```python
import math

import jax
import jax.numpy as jnp
from jax import lax
from jax.sharding import PartitionSpec as P


def rotate(field):
    dim_full = field.shape[-1]
    dim_half = dim_full // 2
    inverse = 1.0 / 10000.0 ** (jnp.arange(0, dim_full, 2, dtype=jnp.float32) / dim_full)
    angles = jnp.arange(field.shape[-4], dtype=jnp.float32)[:, None] * inverse[None, :]
    cosine = jnp.cos(angles)[:, None, None, :]
    sine_table = jnp.sin(angles)[:, None, None, :]
    floats = field.astype(jnp.float32)
    front_part = floats[..., :dim_half]
    second = floats[..., dim_half:]
    turned = jnp.concatenate(
        [front_part * cosine - second * sine_table, second * cosine + front_part * sine_table],
        axis=-1,
    )
    return turned.astype(jnp.bfloat16)


def rms_scale(values, epsilon):
    return values * lax.rsqrt(jnp.mean(values * values, axis=-1, keepdims=True) + epsilon)


def local(
    queries,
    key_rows,
    value_rows,
    lambdas,
    head_gain,
    out_weight,
    residual,
    mixer_gain,
    channel_gain,
    expert_gain,
    routes,
    route_logits,
    gate_weight,
    up_weight,
    down_weight,
):
    head_count = lambdas.shape[0]
    head_dim = head_gain.shape[0] // 2
    seq_query, seq_keys, seq_values = (
        lax.all_to_all(queries, "sp", split_axis=2, concat_axis=1, tiled=True),
        lax.all_to_all(key_rows, "sp", split_axis=2, concat_axis=1, tiled=True),
        lax.all_to_all(value_rows, "sp", split_axis=2, concat_axis=1, tiled=True),
    )
    length = seq_query.shape[1]
    query_rot = rotate(seq_query.reshape(length, head_count, 2, head_dim))
    keys_rot = rotate(seq_keys.reshape(length, head_count, 2, head_dim))
    values_heads = seq_values.reshape(length, head_count, 2 * head_dim)
    block_rows = math.gcd(length, 256)
    query_blocks = query_rot.reshape(length // block_rows, block_rows, head_count, 2, head_dim)
    scale = head_dim ** (-0.5)

    def one_block(query_block):
        scores = (
            jnp.einsum("qhcd,khcd->hcqk", query_block, keys_rot, preferred_element_type=jnp.float32)
            * scale
        )
        probs = jax.nn.softmax(scores, axis=-1)
        mixing = (probs[:, 0] - lambdas[:, None, None] * probs[:, 1]).astype(jnp.bfloat16)
        head_mix = jnp.einsum(
            "hqk,khv->qhv", mixing, values_heads, preferred_element_type=jnp.float32
        )
        return (rms_scale(head_mix, 1e-05) * head_gain).astype(jnp.bfloat16)

    head_out = lax.map(one_block, query_blocks).reshape(1, length, head_count * 2 * head_dim)
    token_rows = lax.all_to_all(head_out, "sp", split_axis=1, concat_axis=2, tiled=True)
    tokens = residual.shape[1]
    model_dim = residual.shape[2]
    projected = jnp.dot(
        token_rows.reshape(tokens, -1), out_weight, preferred_element_type=jnp.float32
    )
    stream = (
        residual.reshape(tokens, model_dim).astype(jnp.float32)
        + rms_scale(projected, 1e-06) * mixer_gain
    ).astype(jnp.bfloat16)
    normed = (rms_scale(stream.astype(jnp.float32), 1e-06) * channel_gain).astype(jnp.bfloat16)
    sp_count = lax.axis_size("sp")
    expert_count = sp_count * gate_weight.shape[0]
    capacity = max(2, 3 * tokens // expert_count)
    top_count = routes.shape[2]
    choice_ids = routes.reshape(-1)
    slots_all = choice_ids.shape[0]
    one_hot = (choice_ids[:, None] == jnp.arange(expert_count, dtype=jnp.int32)[None, :]).astype(
        jnp.int32
    )
    running = jnp.cumsum(one_hot, axis=0)
    slot_index = jnp.sum(one_hot * running, axis=1) - 1
    target = choice_ids * capacity + slot_index
    source_rows = jnp.arange(slots_all, dtype=jnp.int32) // top_count
    outgoing = (
        jnp.zeros((expert_count * capacity, model_dim), jnp.bfloat16)
        .at[target]
        .set(normed[source_rows])
    )
    outgoing = outgoing.reshape(expert_count, capacity, model_dim)
    arrived = lax.all_to_all(outgoing, "sp", split_axis=0, concat_axis=0, tiled=True).reshape(
        sp_count, 1, capacity, model_dim
    )
    expert_arrived = lax.all_gather(arrived, "dp", axis=1, tiled=True)
    shape_in = expert_arrived.shape
    flat_rows = expert_arrived.reshape(-1, shape_in[-1])
    gate_act = jnp.dot(flat_rows, gate_weight[0], preferred_element_type=jnp.float32)
    up_act = jnp.dot(flat_rows, up_weight[0], preferred_element_type=jnp.float32)
    hidden = (jax.nn.silu(gate_act) * up_act).astype(jnp.bfloat16)
    part = jnp.dot(hidden, down_weight[0], preferred_element_type=jnp.float32).astype(jnp.bfloat16)
    partial_value = part.reshape(shape_in)
    summed = lax.psum_scatter(
        partial_value.astype(jnp.float32).astype(jnp.bfloat16),
        "dp",
        scatter_dimension=1,
        tiled=True,
    )
    returned = lax.all_to_all(summed, "sp", split_axis=0, concat_axis=0, tiled=True).reshape(
        expert_count * capacity, model_dim
    )
    picked = returned[target].astype(jnp.float32).reshape(tokens, top_count, model_dim)
    shares = jax.nn.softmax(route_logits.reshape(tokens, top_count), axis=-1)
    combined = jnp.sum(picked * shares[:, :, None], axis=1)
    updated = stream.astype(jnp.float32) + rms_scale(combined, 1e-06) * expert_gain
    return updated.astype(jnp.bfloat16).reshape(1, tokens, model_dim)


def solution(mesh):
    placed = (
        P("dp", "sp", None),
        P("dp", "sp", None),
        P("dp", "sp", None),
        P("sp"),
        P(),
        P(),
        P("dp", "sp", None),
        P(),
        P(),
        P(),
        P("dp", "sp", None),
        P("dp", "sp", None),
        P("sp", None, "dp"),
        P("sp", None, "dp"),
        P("sp", "dp", None),
    )
    return jax.shard_map(
        local, mesh=mesh, in_specs=placed, out_specs=P("dp", "sp", None), check_vma=False
    )
```

profile of v0, /device:TPU:0, one launch (start us, length us, event | category | flops | bytes accessed | tf_op | source)
XLA Modules:
  0.0 448.2 jit_solution(8292478884959336948)
XLA Ops:
  9.5 11.5 %reduce.4 = bf16[2048,128]{1,0:T(8,128)(2,1)S(1)} reduce(bf16[2048,1,128]{2,1,0:T(2,128)(2,1)S(1)} %bitcast.147, bf16[]{:T(256)} %broadcast.286), dimensions={1}, to_apply=%bitcast.104.reduce_sub_computation | reduce | bytes 1048578
  22.0 7.3 %all-to-all-start = ((bf16[8,2,16384]{2,1,0:T(2,128)(2,1)}), bf16[8,2,16384]{2,1,0:T(2,128)(2,1)S(1)}, u32[]{:S(2)}, u32[]{:S(2)}) async-start(bf16[8,2,16384]{2,1,0:T(2,128)(2,1)} %reshape.320), calls=%async_computation | async-start | bytes 1048576 | tf_op jit(solution)/shard_map/all_to_all | solution.py:50
  30.0 11.5 %reduce.3 = bf16[2048,128]{1,0:T(8,128)(2,1)S(1)} reduce(bf16[2048,1,128]{2,1,0:T(2,128)(2,1)S(1)} %bitcast.151, bf16[]{:T(256)} %broadcast.286), dimensions={1}, to_apply=%bitcast.106.reduce_sub_computation | reduce | bytes 1048578
  43.7 4.9 %all-to-all-start.1 = ((bf16[8,2,16384]{2,1,0:T(2,128)(2,1)}), bf16[8,2,16384]{2,1,0:T(2,128)(2,1)S(1)}, u32[]{:S(2)}, u32[]{:S(2)}) async-start(bf16[8,2,16384]{2,1,0:T(2,128)(2,1)} %reshape.322), calls=%async_computation.1 | async-start | bytes 1048576 | tf_op jit(solution)/shard_map/all_to_all | solution.py:51
  49.4 11.5 %reduce.5 = bf16[2048,128]{1,0:T(8,128)(2,1)S(1)} reduce(bf16[2048,1,128]{2,1,0:T(2,128)(2,1)S(1)} %bitcast.152, bf16[]{:T(256)} %broadcast.286), dimensions={1}, to_apply=%bitcast.108.reduce_sub_computation | reduce | bytes 1048578
  62.7 6.0 %all-to-all-start.2 = ((bf16[8,2,16384]{2,1,0:T(2,128)(2,1)}), bf16[8,2,16384]{2,1,0:T(2,128)(2,1)}, u32[]{:S(2)}, u32[]{:S(2)}) async-start(bf16[8,2,16384]{2,1,0:T(2,128)(2,1)} %reshape.324), calls=%async_computation.2 | async-start | bytes 1048576 | tf_op jit(solution)/shard_map/all_to_all | solution.py:52
  74.6 7.6 %all-to-all-done.2 = bf16[8,2,16384]{2,1,0:T(2,128)(2,1)} async-done(((bf16[8,2,16384]{2,1,0:T(2,128)(2,1)}), bf16[8,2,16384]{2,1,0:T(2,128)(2,1)}, u32[]{:S(2)}, u32[]{:S(2)}) %all-to-all-start.2) | async-done | bytes 524320 | tf_op jit(solution)/shard_map/all_to_all | solution.py:52
  86.9 27.5 %while.10 = (s32[]{:T(128)}, bf16[4,256,2,128]{3,2,1,0:T(2,128)(2,1)S(1)}, bf16[4,256,2,2,64]{1,4,3,2,0:T(8,128)(2,1)S(1)}, bf16[1024,2,2,64]{0,3,2,1:T(8,128)(2...) while((s32[]{:T(128)}, ...), condition=%wide.region_4.5_spmd, body=%wide.region_0.4_spmd.sunk | while | flops 274531840 | bytes 19153508 | solution.py:74
  93.8 3.3 fusion.74
  100.6 3.3 fusion.74
  107.5 3.3 fusion.74
  114.6 3.8 reduce.6
  119.3 3.7 all-to-all-start.3
  123.7 13.1 %all-to-all-done.3 = bf16[8,2,16384]{2,1,0:T(2,128)(2,1)S(1)} async-done(((bf16[8,2,16384]{2,1,0:T(2,128)(2,1)}), bf16[8,2,16384]{2,1,0:T(2,128)(2,1)S(1)}, u32[]{:S(2)}, u32[]{:S(2)}) %all-to-all-start.3) | async-done | bytes 524320 | tf_op jit(solution)/shard_map/all_to_all | solution.py:75
  137.7 4.8 %multiply_reduce_fusion.4 = (f32[128]{0:T(128)S(1)}, f32[128,2048]{1,0:T(8,128)S(1)}) fusion(bf16[128,2048]{0,1:T(8,128)(2,1)S(1)} %bitcast.153, bf16[2048,2048]{1,0:T(8,128)(2,1)} %param.22), kind=kOutput, calls=%fused_computation.50 | convolution fusion | flops 1074265984 | bytes 9961984 | tf_op jit(solution)/shard_map/dot_general | solution.py:78
  143.1 5.9 %scatter_custom_fusion = bf16[384,2048]{1,0:T(8,128)(2,1)S(1)} fusion(s32[256]{0:T(256)S(1)} %bitcast.158, bf16[128,2048]{1,0:T(8,128)(2,1)S(1)} %fusion.38, s32[1024]{0:T(1024)S(1)} %pad_clamp_fusion.1, bf16[]{:T(256)} %constant.64.clone.1), kind=kCustom, calls=%fused_computation.47 | custom fusion | bytes 1572866 | tf_op jit(solution)/shard_map/scatter | solution.py:102
  149.1 39.9 %all_to_all.58 = bf16[8,48,2048]{2,1,0:T(8,128)(2,1)} all-to-all(bf16[8,48,2048]{2,1,0:T(8,128)(2,1)S(1)} %bitcast.144), channel_id=1, replica_groups=mesh['sp'=8,'dp'=4] {'sp'}, dimensions={0} | all-to-all | bytes 3145728 | tf_op jit(solution)/shard_map/all_to_all | solution.py:105
  189.4 45.0 %all-gather.3.cloned.1.call-done = bf16[8,192,2048]{2,1,0:T(8,128)(2,1)} async-done(((bf16[8,48,2048]{2,1,0:T(8,128)(2,1)}), bf16[8,192,2048]{2,1,0:T(8,128)(2,1)}) %all-gather.3.cloned.1.call-update) | async-done | bytes 6291472 | tf_op jit(solution)/shard_map/all_gather | solution.py:108
  234.5 11.6 %fusion.33 = f32[1536,1024]{1,0:T(8,128)} fusion(bf16[1536,2048]{1,0:T(8,128)(2,1)} %bitcast.162, bf16[1,2048,1024]{2,1,0:T(8,128)(2,1)} %param.29), kind=kOutput, calls=%fused_computation.34 | convolution fusion | flops 6442450944 | bytes 16777216 | tf_op jit(solution)/shard_map/dot_general | solution.py:111
  246.1 20.5 %convolution_convert_fusion = bf16[1536,2048]{1,0:T(8,128)(2,1)} fusion(bf16[1,1024,2048]{2,1,0:T(8,128)(2,1)} %param.31, f32[1536,1024]{1,0:T(8,128)} %fusion.33, bf16[1536,2048]{1,0:T(8,128)(2,1)} %bitcast.163, bf16[1,2048,1024]{2,1,0:T(8,128)(2,1)} %param.30), kind=kOutput, calls=%fused_computation.30 | convolution fusion | flops 12897484800 | bytes 27262976 | tf_op jit(solution)/shard_map/dot_general | solution.py:114
  267.9 118.5 %all-reduce.3.cloned.1.call-done = bf16[8,4,48,2048]{3,2,1,0:T(8,128)(2,1)} async-done(((bf16[8,4,48,2048]{3,2,1,0:T(8,128)(2,1)}), bf16[8,4,48,2048]{3,2,1,0:T(8,128)(2,1)}) %all-reduce.3.cloned.1.call-update) | async-done | bytes 6291472
  386.4 3.4 constant_dynamic-slice_fusion
  389.8 5.7 %all-to-all-start.5 = ((bf16[8,1,48,2048]{3,2,1,0:T(8,128)(2,1)}), bf16[8,1,48,2048]{3,2,1,0:T(8,128)(2,1)S(1)}, u32[]{:S(2)}, u32[]{:S(2)}) async-start(bf16[8,1,48,2048]{3,2,1,0:T(8,128)(2,1)} %constant_dynamic-slice_fusion), calls=%async_computation.5 | async-start | bytes 3145728 | tf_op jit(solution)/shard_map/all_to_all | solution.py:122
  395.7 36.4 %all-to-all-done.5 = bf16[8,1,48,2048]{3,2,1,0:T(8,128)(2,1)S(1)} async-done(((bf16[8,1,48,2048]{3,2,1,0:T(8,128)(2,1)}), bf16[8,1,48,2048]{3,2,1,0:T(8,128)(2,1)S(1)}, u32[]{:S(2)}, u32[]{:S(2)}) %all-to-all-start.5) | async-done | bytes 1572896 | tf_op jit(solution)/shard_map/all_to_all | solution.py:122
  (123 shorter events, 51.4 us)
Async XLA Ops:
  6.5 22.7 %copy-start = (bf16[1,128,2048]{2,1,0:T(8,128)(2,1)S(1)}, bf16[1,128,2048]{2,1,0:T(8,128)(2,1)}, u32[]{:S(2)}) copy-start(bf16[1,128,2048]{2,1,0:T(8,128)(2,1)} %param.18) | copy-start | bytes 1572868
  9.5 39.1 %copy-start.1 = (bf16[1,128,2048]{2,1,0:T(8,128)(2,1)S(1)}, bf16[1,128,2048]{2,1,0:T(8,128)(2,1)}, u32[]{:S(2)}) copy-start(bf16[1,128,2048]{2,1,0:T(8,128)(2,1)} %param.19) | copy-start | bytes 1572868
  22.0 21.8 %all-to-all-start = ((bf16[8,2,16384]{2,1,0:T(2,128)(2,1)}), bf16[8,2,16384]{2,1,0:T(2,128)(2,1)S(1)}, u32[]{:S(2)}, u32[]{:S(2)}) async-start(bf16[8,2,16384]{2,1,0:T(2,128)(2,1)} %reshape.320), calls=%async_computation | async-start | bytes 1048576 | tf_op jit(solution)/shard_map/all_to_all | solution.py:50
  30.0 31.8 %copy-start.11 = (s32[1,128,2]{1,2,0:T(2,128)S(1)}, s32[1,128,2]{1,2,0:T(2,128)}, u32[]{:S(2)}) copy-start(s32[1,128,2]{1,2,0:T(2,128)} %param.27) | copy-start | bytes 3076
  43.7 18.9 %all-to-all-start.1 = ((bf16[8,2,16384]{2,1,0:T(2,128)(2,1)}), bf16[8,2,16384]{2,1,0:T(2,128)(2,1)S(1)}, u32[]{:S(2)}, u32[]{:S(2)}) async-start(bf16[8,2,16384]{2,1,0:T(2,128)(2,1)} %reshape.322), calls=%async_computation.1 | async-start | bytes 1048576 | tf_op jit(solution)/shard_map/all_to_all | solution.py:51
  62.7 19.5 %all-to-all-start.2 = ((bf16[8,2,16384]{2,1,0:T(2,128)(2,1)}), bf16[8,2,16384]{2,1,0:T(2,128)(2,1)}, u32[]{:S(2)}, u32[]{:S(2)}) async-start(bf16[8,2,16384]{2,1,0:T(2,128)(2,1)} %reshape.324), calls=%async_computation.2 | async-start | bytes 1048576 | tf_op jit(solution)/shard_map/all_to_all | solution.py:52
  69.1 3.6 copy-start.10
  84.4 1.9 copy-start.2
  84.5 1.9 copy-start.5
  84.5 1.9 copy-start.12
  85.8 1.0 copy-start.3
  114.3 9.2 %slice-start = ((s32[8,3]{0,1:T(4,128)}), s32[8,2]{0,1:T(2,128)S(1)}, s32[]{:S(2)}) async-start(s32[8,3]{0,1:T(4,128)} %copy-done.10), calls=%async_computation.8 | async-start | bytes 2048 | tf_op jit(solution)/shard_map/slice.1
  119.3 17.5 %all-to-all-start.3 = ((bf16[8,2,16384]{2,1,0:T(2,128)(2,1)}), bf16[8,2,16384]{2,1,0:T(2,128)(2,1)S(1)}, u32[]{:S(2)}, u32[]{:S(2)}) async-start(bf16[8,2,16384]{2,1,0:T(2,128)(2,1)} %reshape.326), calls=%async_computation.3 | async-start | bytes 1048576 | tf_op jit(solution)/shard_map/all_to_all | solution.py:75
  123.0 111.5 %all-gather.3.cloned.1.call-start = ((), (), s32[]{:S(2)}) async-start(), calls=%async_computation.6 | async-start | bytes 7864320 | tf_op jit(solution)/shard_map/all_gather | solution.py:108
  137.7 4.8 %copy-start.4 = (bf16[1,128,2048]{2,1,0:T(8,128)(2,1)S(1)}, bf16[1,128,2048]{2,1,0:T(8,128)(2,1)}, u32[]{:S(2)}) copy-start(bf16[1,128,2048]{2,1,0:T(8,128)(2,1)} %param.23) | copy-start | bytes 1572868
  137.7 4.8 %copy-start.7 = (f32[2048]{0:T(1024)S(1)}, f32[2048]{0:T(1024)}, u32[]{:S(2)}) copy-start(f32[2048]{0:T(1024)} %param.24) | copy-start | bytes 24580
  137.7 5.2 %copy-start.8 = (f32[2048]{0:T(1024)S(1)}, f32[2048]{0:T(1024)}, u32[]{:S(2)}) copy-start(f32[2048]{0:T(1024)} %param.25) | copy-start | bytes 24580
  189.0 197.4 %all-reduce.3.cloned.1.call-start = ((), (), s32[]{:S(2)}) async-start(), calls=%async_computation.7 | async-start | bytes 12582912
  266.6 0.7 copy-start.13
  266.7 128.9 %copy-start.6 = (f32[1,128,2]{1,2,0:T(2,128)S(1)}, f32[1,128,2]{1,2,0:T(2,128)}, u32[]{:S(2)}) copy-start(f32[1,128,2]{1,2,0:T(2,128)} %param.28) | copy-start | bytes 3076
  389.8 42.3 %all-to-all-start.5 = ((bf16[8,1,48,2048]{3,2,1,0:T(8,128)(2,1)}), bf16[8,1,48,2048]{3,2,1,0:T(8,128)(2,1)S(1)}, u32[]{:S(2)}, u32[]{:S(2)}) async-start(bf16[8,1,48,2048]{3,2,1,0:T(8,128)(2,1)} %constant_dynamic-slice_fusion), calls=%async_computation.5 | async-start | bytes 3145728 | tf_op jit(solution)/shard_map/all_to_all | solution.py:122
  434.4 5.7 %copy-start.9 = (f32[2048]{0:T(1024)S(1)}, f32[2048]{0:T(1024)}, u32[]{:S(2)}) copy-start(f32[2048]{0:T(1024)} %param.26) | copy-start | bytes 24580
Sparse Core Ops, SparseCore 0:
  189.1 45.3 all-gather.2
  266.8 119.5 all-reduce.2
where the time goes:
time: 457 us; the launch traced here: 448 us
  waiting for transfers between devices  222 us (49%)
  other arithmetic  58.1 us (13%)
  matrix products  52.5 us (11%)
  blocking collectives  39.9 us (9%)
  local copies, waits for them, and re-layouts  33.3 us (7%)
  starting transfers between devices  28.3 us (6%)
  between operations  14.1 us (3%)
    unnamed x3, waiting for transfers between devices  119 us
    all_gather x1, waiting for transfers between devices, local(): expert_arrived = lax.all_gather(arrived, 'dp', axis=1, tiled=True)  45 us
    all_to_all x1, blocking collectives, local(): lax.all_to_all(outgoing, 'sp', split_axis=0, concat_axis=0, tiled=True)  39.9 us
    unnamed x4, other arithmetic  38.3 us
    all_to_all x1, waiting for transfers between devices, local(): lax.all_to_all(summed, 'sp', split_axis=0, concat_axis=0, tiled=True)  36.4 us
    dot_general x1, matrix products, local(): jnp.dot(hidden, down_weight[0], preferred_element_type=jnp.float32)  20.5 us
    unnamed x45, local copies, waits for them, and re-layouts  17.4 us
    sub x4, matrix products, one_block(): probs = jax.nn.softmax(scores, axis=-1)  13.2 us
  transfers between devices with their start and end apart: 7, of which 6 were waited for; matrix products, arithmetic and copies ran while one was open for 8% of the time, Pallas kernels for 0%

commit v1 on v0

--- a/solution.py
+++ b/solution.py
@@ -1,8 +1,11 @@
+import functools
 import math
 
 import jax
 import jax.numpy as jnp
 from jax import lax
+from jax.experimental import pallas as pl
+from jax.experimental.pallas import tpu as pltpu
 from jax.sharding import PartitionSpec as P
 
 
@@ -25,6 +28,311 @@
 
 def rms_scale(values, epsilon):
     return values * lax.rsqrt(jnp.mean(values * values, axis=-1, keepdims=True) + epsilon)
+
+
+MESH = pl.DeviceIdType.MESH
+
+
+def expert_kernel(
+    count,
+    groups,
+    rows_ref,
+    place_ref,
+    mix_ref,
+    stream_ref,
+    gain_ref,
+    gate_hbm,
+    up_hbm,
+    down_hbm,
+    out_ref,
+    outgoing,
+    arrived,
+    own,
+    pair_in,
+    cross_in,
+    final,
+    returned,
+    hidden,
+    gate_w,
+    up_w,
+    down_w,
+    w_sem,
+    a_send,
+    a_recv,
+    b_send,
+    b_recv,
+    c_send,
+    c_recv,
+    d_send,
+    d_recv,
+    e_send,
+    e_recv,
+    f_send,
+    f_recv,
+):
+    me = lax.axis_index("sp")
+    dp = lax.axis_index("dp")
+    chip, core = dp // 2, dp % 2
+    other = {"sp": me, "dp": chip * 2 + (1 - core)}
+
+    def chip_at(step):
+        return {"sp": me, "dp": ((chip + step + groups) % groups) * 2 + core}
+
+    def sp_at(step):
+        return {"sp": (me + step + count) % count, "dp": dp}
+
+    def remote(src, dst, send, recv, device):
+        return pltpu.make_async_remote_copy(
+            src_ref=src, dst_ref=dst, send_sem=send, recv_sem=recv, device_id=device, device_id_type=MESH
+        )
+
+    def send_out(k):
+        return remote(outgoing.at[k], arrived.at[k, 0, 0], a_send.at[k], a_recv.at[k], sp_at(k))
+
+    def cross_out(k, j):
+        return remote(arrived.at[k, 0, 0], arrived.at[k, 0, j], b_send.at[k, j], b_recv.at[k, j], chip_at(j))
+
+    def twin_out(k, j):
+        return remote(arrived.at[k, 0, j], arrived.at[k, 1, j], c_send.at[k, j], c_recv.at[k, j], other)
+
+    def pair_out(k):
+        return remote(arrived.at[k, 1], pair_in.at[k], d_send.at[k], d_recv.at[k], other)
+
+    def cross_back(k, j):
+        return remote(own.at[k, j], cross_in.at[k, j], e_send.at[k, j], e_recv.at[k, j], chip_at(-j))
+
+    def send_back(k):
+        return remote(final.at[k], returned.at[k], f_send.at[k], f_recv.at[k], sp_at(-k))
+
+    weights = [
+        pltpu.make_async_copy(hbm, vmem, w_sem.at[i])
+        for i, (hbm, vmem) in enumerate(((gate_hbm, gate_w), (up_hbm, up_w), (down_hbm, down_w)))
+    ]
+    for copy in weights:
+        copy.start()
+
+    barrier = pltpu.get_barrier_semaphore()
+    peers = [sp_at(k) for k in range(1, count)] + [chip_at(j) for j in range(1, groups)] + [other]
+    for peer in peers:
+        pl.semaphore_signal(barrier, inc=1, device_id=peer, device_id_type=MESH)
+
+    capacity = outgoing.shape[1]
+    model = rows_ref.shape[1]
+    units = gate_w.shape[1]
+    wide = math.gcd(model, 512)
+
+    @pl.loop(0, model // wide)
+    def _(n):
+        cols = pl.ds(pl.multiple_of(n * wide, wide), wide)
+        block = jnp.dot(place_ref[...], rows_ref[:, cols], preferred_element_type=jnp.float32)
+        block = block.astype(jnp.bfloat16).reshape(count, capacity, wide)
+        arrived[0, 0, 0, :, cols] = block[0]
+        outgoing[:, :, cols] = block
+
+    pl.semaphore_wait(barrier, len(peers))
+
+    @pl.loop(1, count)
+    def _(k):
+        send_out(k).start()
+
+    width = 2
+    rounds = count // width
+
+    def per_k(group, action):
+        for i in range(width):
+            action(group * width + i)
+
+    def forward(k):
+        @pl.when(k > 0)
+        def _():
+            send_out(k).wait_recv()
+
+        for j in range(1, groups):
+            cross_out(k, j).start()
+        twin_out(k, 0).start()
+
+    def forward_twin(k):
+        for j in range(1, groups):
+            cross_out(k, j).wait_recv()
+            twin_out(k, j).start()
+
+    def complete(k):
+        for j in range(groups):
+            twin_out(k, j).wait_recv()
+
+    def pair_sum(k):
+        pair_out(k).wait_recv()
+        for j in range(groups):
+            own[k, j] = (own[k, j].astype(jnp.float32) + pair_in[k, j].astype(jnp.float32)).astype(jnp.bfloat16)
+        for j in range(1, groups):
+            cross_back(k, j).start()
+
+    def total(k):
+        value = own[k, 0].astype(jnp.float32)
+        for j in range(1, groups):
+            cross_back(k, j).wait_recv()
+            value = value + cross_in[k, j].astype(jnp.float32)
+        value = value.astype(jnp.bfloat16)
+
+        @pl.when(k > 0)
+        def _():
+            final[k] = value
+            send_back(k).start()
+
+        @pl.when(k == 0)
+        def _():
+            returned[k] = value
+
+    tile = math.gcd(units, 256)
+
+    def compute(group):
+        first = group * width
+        held = width * 2 * groups * capacity
+        slab = arrived.at[pl.ds(first, width)]
+
+        @pl.loop(0, units // tile)
+        def _(n):
+            cols = pl.ds(pl.multiple_of(n * tile, tile), tile)
+            value = slab[...].reshape(held, model)
+            gate = jnp.dot(value, gate_w[:, cols], preferred_element_type=jnp.float32)
+            up = jnp.dot(value, up_w[:, cols], preferred_element_type=jnp.float32)
+            hidden[:, cols] = (gate / (1.0 + jnp.exp(-gate)) * up).astype(jnp.bfloat16)
+
+        @pl.loop(0, model // wide)
+        def _(n):
+            cols = pl.ds(pl.multiple_of(n * wide, wide), wide)
+            part = jnp.dot(hidden[...], down_w[:, cols], preferred_element_type=jnp.float32)
+            part = part.astype(jnp.bfloat16).reshape(width, 2, groups, capacity, wide)
+            for i in range(width):
+                own[first + i, :, :, cols] = part[i, 0]
+                arrived[first + i, 1, :, :, cols] = part[i, 1]
+
+        per_k(group, lambda k: pair_out(k).start())
+
+    @pl.loop(0, rounds + 3)
+    def _(g):
+        @pl.when(g < rounds)
+        def _():
+            per_k(g, forward)
+
+        @pl.when((g >= 2) & (g < rounds + 2))
+        def _():
+            per_k(g - 2, pair_sum)
+
+        @pl.when(g >= 3)
+        def _():
+            per_k(g - 3, total)
+
+        @pl.when((g >= 1) & (g < rounds + 1))
+        def _():
+            @pl.when(g == 1)
+            def _():
+                for copy in weights:
+                    copy.wait()
+
+            per_k(g - 1, forward_twin)
+            per_k(g - 1, complete)
+            compute(g - 1)
+
+    @pl.loop(1, count)
+    def _(k):
+        send_back(k).wait_recv()
+
+    square = jnp.zeros((stream_ref.shape[0], 1), jnp.float32)
+    share = mix_ref[...]
+    high = share.astype(jnp.bfloat16)
+    low = (share - high.astype(jnp.float32)).astype(jnp.bfloat16)
+    pieces = []
+    for n in range(model // wide):
+        cols = slice(n * wide, (n + 1) * wide)
+        back = returned[:, :, cols].reshape(count * capacity, wide)
+        piece = jnp.dot(high, back, preferred_element_type=jnp.float32)
+        piece = piece + jnp.dot(low, back, preferred_element_type=jnp.float32)
+        square = square + jnp.sum(piece * piece, axis=-1, keepdims=True)
+        pieces.append(piece)
+    norm = lax.rsqrt(square / model + 1e-06)
+    for n, piece in enumerate(pieces):
+        cols = slice(n * wide, (n + 1) * wide)
+        value = stream_ref[:, cols].astype(jnp.float32) + piece * norm * gain_ref[:, cols]
+        out_ref[:, cols] = value.astype(jnp.bfloat16)
+
+    @pl.loop(0, count)
+    def _(k):
+        @pl.when(k > 0)
+        def _():
+            send_out(k).wait_send()
+            send_back(k).wait_send()
+
+        for j in range(1, groups):
+            cross_out(k, j).wait_send()
+            cross_back(k, j).wait_send()
+        for j in range(groups):
+            twin_out(k, j).wait_send()
+        pair_out(k).wait_send()
+
+
+def expert_stage(normed, stream, routes, logits, expert_gain, gate_weight, up_weight, down_weight):
+    count, dp_count = lax.axis_size("sp"), lax.axis_size("dp")
+    groups = dp_count // 2
+    tokens, model = normed.shape
+    units = gate_weight.shape[1]
+    top = routes.shape[1]
+    capacity = -(-max(2, 3 * tokens // count) // 16) * 16
+    relative = (routes - lax.axis_index("sp") + count) % count
+    flat = relative.reshape(-1)
+    one_hot = (flat[:, None] == jnp.arange(count, dtype=jnp.int32)[None, :]).astype(jnp.float32)
+    slots = tokens * top
+    lower = (jnp.arange(slots)[:, None] >= jnp.arange(slots)[None, :]).astype(jnp.float32)
+    running = jnp.dot(lower, one_hot, preferred_element_type=jnp.float32)
+    slot = jnp.sum(one_hot * running, axis=1).astype(jnp.int32) - 1
+    target = (flat * capacity + slot).reshape(tokens, top)
+    shares = jax.nn.softmax(logits, axis=-1)
+    places = jnp.arange(count * capacity, dtype=jnp.int32)
+    mix = jnp.zeros((tokens, count * capacity), jnp.float32)
+    place = jnp.zeros((count * capacity, tokens), jnp.bool_)
+    for i in range(top):
+        mix = mix + jnp.where(target[:, i, None] == places[None, :], shares[:, i, None], 0.0)
+        place = place | (target[None, :, i] == places[:, None])
+    place = place.astype(jnp.bfloat16)
+    vmem, anywhere = pl.BlockSpec(memory_space=pltpu.VMEM), pl.BlockSpec(memory_space=pl.ANY)
+    half = jnp.bfloat16
+    dma = pltpu.SemaphoreType.DMA
+    return pl.pallas_call(
+        functools.partial(expert_kernel, count, groups),
+        out_shape=jax.ShapeDtypeStruct((tokens, model), jnp.bfloat16),
+        in_specs=[vmem] * 5 + [anywhere] * 3,
+        out_specs=vmem,
+        scratch_shapes=[
+            pltpu.VMEM((count, capacity, model), half),
+            pltpu.VMEM((count, 2, groups, capacity, model), half),
+            pltpu.VMEM((count, groups, capacity, model), half),
+            pltpu.VMEM((count, groups, capacity, model), half),
+            pltpu.VMEM((count, groups, capacity, model), half),
+            pltpu.VMEM((count, capacity, model), half),
+            pltpu.VMEM((count, capacity, model), half),
+            pltpu.VMEM((4 * groups * capacity, units), half),
+            pltpu.VMEM((model, units), half),
+            pltpu.VMEM((model, units), half),
+            pltpu.VMEM((units, model), half),
+            dma((3,)),
+            dma((count,)),
+            dma((count,)),
+            dma((count, groups)),
+            dma((count, groups)),
+            dma((count, groups)),
+            dma((count, groups)),
+            dma((count,)),
+            dma((count,)),
+            dma((count, groups)),
+            dma((count, groups)),
+            dma((count,)),
+            dma((count,)),
+        ],
+        compiler_params=pltpu.CompilerParams(
+            collective_id=1, has_side_effects=True, vmem_limit_bytes=67043328
+        ),
+        name="experts",
+    )(normed, place, mix, stream, expert_gain[None, :], gate_weight, up_weight, down_weight)
 
 
 def local(
@@ -83,50 +391,17 @@
         + rms_scale(projected, 1e-06) * mixer_gain
     ).astype(jnp.bfloat16)
     normed = (rms_scale(stream.astype(jnp.float32), 1e-06) * channel_gain).astype(jnp.bfloat16)
-    sp_count = lax.axis_size("sp")
-    expert_count = sp_count * gate_weight.shape[0]
-    capacity = max(2, 3 * tokens // expert_count)
-    top_count = routes.shape[2]
-    choice_ids = routes.reshape(-1)
-    slots_all = choice_ids.shape[0]
-    one_hot = (choice_ids[:, None] == jnp.arange(expert_count, dtype=jnp.int32)[None, :]).astype(
-        jnp.int32
-    )
-    running = jnp.cumsum(one_hot, axis=0)
-    slot_index = jnp.sum(one_hot * running, axis=1) - 1
-    target = choice_ids * capacity + slot_index
-    source_rows = jnp.arange(slots_all, dtype=jnp.int32) // top_count
-    outgoing = (
-        jnp.zeros((expert_count * capacity, model_dim), jnp.bfloat16)
-        .at[target]
-        .set(normed[source_rows])
-    )
-    outgoing = outgoing.reshape(expert_count, capacity, model_dim)
-    arrived = lax.all_to_all(outgoing, "sp", split_axis=0, concat_axis=0, tiled=True).reshape(
-        sp_count, 1, capacity, model_dim
-    )
-    expert_arrived = lax.all_gather(arrived, "dp", axis=1, tiled=True)
-    shape_in = expert_arrived.shape
-    flat_rows = expert_arrived.reshape(-1, shape_in[-1])
-    gate_act = jnp.dot(flat_rows, gate_weight[0], preferred_element_type=jnp.float32)
-    up_act = jnp.dot(flat_rows, up_weight[0], preferred_element_type=jnp.float32)
-    hidden = (jax.nn.silu(gate_act) * up_act).astype(jnp.bfloat16)
-    part = jnp.dot(hidden, down_weight[0], preferred_element_type=jnp.float32).astype(jnp.bfloat16)
-    partial_value = part.reshape(shape_in)
-    summed = lax.psum_scatter(
-        partial_value.astype(jnp.float32).astype(jnp.bfloat16),
-        "dp",
-        scatter_dimension=1,
-        tiled=True,
-    )
-    returned = lax.all_to_all(summed, "sp", split_axis=0, concat_axis=0, tiled=True).reshape(
-        expert_count * capacity, model_dim
-    )
-    picked = returned[target].astype(jnp.float32).reshape(tokens, top_count, model_dim)
-    shares = jax.nn.softmax(route_logits.reshape(tokens, top_count), axis=-1)
-    combined = jnp.sum(picked * shares[:, :, None], axis=1)
-    updated = stream.astype(jnp.float32) + rms_scale(combined, 1e-06) * expert_gain
-    return updated.astype(jnp.bfloat16).reshape(1, tokens, model_dim)
+    updated = expert_stage(
+        normed,
+        stream,
+        routes.reshape(tokens, -1),
+        route_logits.reshape(tokens, -1),
+        expert_gain,
+        gate_weight[0],
+        up_weight[0],
+        down_weight[0],
+    )
+    return updated.reshape(1, tokens, model_dim)
 
 
 def solution(mesh):

time: 457 us -> 268 us (0.59); the launches traced: 448 us -> 267 us
  waiting for transfers between devices: 222 us -> 33.9 us
  Pallas kernels: 0 us -> 116 us
  blocking collectives: 39.9 us -> 0 us
  matrix products: 52.5 us -> 20.5 us
  between operations: 14.1 us -> 0.44 us
  local copies, waits for them, and re-layouts: 33.3 us -> 20.2 us
  starting transfers between devices: 28.3 us -> 21.4 us
    unnamed x3 -> x0, waiting for transfers between devices: 119 us -> none
    pallas_call x0 -> x1, Pallas kernels: none -> 116 us  [expert_stage(): pl.pallas_call(functools.partial(expert_kernel, count, groups), out_shape...]
    all_gather x1 -> x0, waiting for transfers between devices: 45 us -> none  [local(): expert_arrived = lax.all_gather(arrived, 'dp', axis=1, tiled=True)]
    all_to_all x1 -> x0, blocking collectives: 39.9 us -> none  [local(): lax.all_to_all(outgoing, 'sp', split_axis=0, concat_axis=0, tiled=True)]
    all_to_all x1 -> x0, waiting for transfers between devices: 36.4 us -> none  [local(): lax.all_to_all(summed, 'sp', split_axis=0, concat_axis=0, tiled=True)]
    dot_general x2 -> x1, matrix products: 32.2 us -> 0.2 us  [expert_stage(): running = jnp.dot(lower, one_hot, preferred_element_type=jnp.float32)]
    all_to_all x1, waiting for transfers between devices: 0.01 us -> 13.2 us  [local(): lax.all_to_all(key_rows, 'sp', split_axis=2, concat_axis=1, tiled=True)]
    scatter x1 -> x0, local copies, waits for them, and re-layouts: 5.92 us -> none  [local(): outgoing = jnp.zeros((expert_count * capacity, model_dim), jnp.bfloat16)....]
  transfers between devices with their start and end apart: 7 -> 4, of which waited for: 6 -> 3; matrix products, arithmetic and copies ran while one was open for 8% -> 13% of each run, Pallas kernels for 0% -> 0%
where the time goes in v1:
time: 268 us; the launch traced here: 267 us
  Pallas kernels  116 us (43%)
  other arithmetic  55.3 us (21%)
  waiting for transfers between devices  33.9 us (13%)
  starting transfers between devices  21.4 us (8%)
  matrix products  20.5 us (8%)
  local copies, waits for them, and re-layouts  20.2 us (8%)
    pallas_call x1, Pallas kernels, expert_stage(): pl.pallas_call(functools.partial(expert_kernel, count, groups), out_shape...  116 us
    unnamed x4, other arithmetic  38.3 us
    unnamed x39, local copies, waits for them, and re-layouts  15.3 us
    all_to_all x1, waiting for transfers between devices, local(): lax.all_to_all(key_rows, 'sp', split_axis=2, concat_axis=1, tiled=True)  13.2 us
    sub x4, matrix products, one_block(): probs = jax.nn.softmax(scores, axis=-1)  13.2 us
    all_to_all x1, waiting for transfers between devices, local(): lax.all_to_all(head_out, 'sp', split_axis=1, concat_axis=2, tiled=True)  12.5 us
    div x4, other arithmetic, one_block(): probs = jax.nn.softmax(scores, axis=-1)  10.5 us
    all_to_all x1, waiting for transfers between devices, local(): lax.all_to_all(value_rows, 'sp', split_axis=2, concat_axis=1, tiled=True)  8.11 us
  transfers between devices with their start and end apart: 4, of which 3 were waited for; matrix products, arithmetic and copies ran while one was open for 13% of the time, Pallas kernels for 0%

profile of v1, /device:TPU:0, one launch (start us, length us, event | category | flops | bytes accessed | tf_op | source)
XLA Modules:
  0.0 267.5 jit_solution(12357084399677999698)
XLA Ops:
  0.0 2.4 copy.83
  2.9 11.5 %reduce.2 = bf16[2048,128]{1,0:T(8,128)(2,1)S(1)} reduce(bf16[2048,1,128]{2,1,0:T(2,128)(2,1)S(1)} %bitcast.127, bf16[]{:T(256)} %broadcast.186), dimensions={1}, to_apply=%bitcast.86.reduce_sub_computation | reduce | bytes 1048578
  15.4 7.3 %all-to-all-start = ((bf16[8,2,16384]{2,1,0:T(2,128)(2,1)}), bf16[8,2,16384]{2,1,0:T(2,128)(2,1)S(1)}, u32[]{:S(2)}, u32[]{:S(2)}) async-start(bf16[8,2,16384]{2,1,0:T(2,128)(2,1)} %reshape.156), calls=%async_computation | async-start | bytes 1048576 | tf_op jit(solution)/shard_map/all_to_all | solution.py:358
  23.4 11.5 %reduce.1 = bf16[2048,128]{1,0:T(8,128)(2,1)S(1)} reduce(bf16[2048,1,128]{2,1,0:T(2,128)(2,1)S(1)} %bitcast.131, bf16[]{:T(256)} %broadcast.186), dimensions={1}, to_apply=%bitcast.88.reduce_sub_computation | reduce | bytes 1048578
  36.6 11.5 %reduce.3 = bf16[2048,128]{1,0:T(8,128)(2,1)S(1)} reduce(bf16[2048,1,128]{2,1,0:T(2,128)(2,1)S(1)} %bitcast.132, bf16[]{:T(256)} %broadcast.186), dimensions={1}, to_apply=%bitcast.90.reduce_sub_computation | reduce | bytes 1048578
  49.1 6.0 %all-to-all-start.1 = ((bf16[8,2,16384]{2,1,0:T(2,128)(2,1)}), bf16[8,2,16384]{2,1,0:T(2,128)(2,1)S(1)}, u32[]{:S(2)}, u32[]{:S(2)}) async-start(bf16[8,2,16384]{2,1,0:T(2,128)(2,1)} %reshape.158), calls=%async_computation.1 | async-start | bytes 1048576 | tf_op jit(solution)/shard_map/all_to_all | solution.py:359
  55.8 13.2 %all-to-all-done.1 = bf16[8,2,16384]{2,1,0:T(2,128)(2,1)S(1)} async-done(((bf16[8,2,16384]{2,1,0:T(2,128)(2,1)}), bf16[8,2,16384]{2,1,0:T(2,128)(2,1)S(1)}, u32[]{:S(2)}, u32[]{:S(2)}) %all-to-all-start.1) | async-done | bytes 524320 | tf_op jit(solution)/shard_map/all_to_all | solution.py:359
  69.0 4.4 %all-to-all-start.2 = ((bf16[8,2,16384]{2,1,0:T(2,128)(2,1)}), bf16[8,2,16384]{2,1,0:T(2,128)(2,1)}, u32[]{:S(2)}, u32[]{:S(2)}) async-start(bf16[8,2,16384]{2,1,0:T(2,128)(2,1)} %reshape.160), calls=%async_computation.2 | async-start | bytes 1048576 | tf_op jit(solution)/shard_map/all_to_all | solution.py:360
  78.9 8.1 %all-to-all-done.2 = bf16[8,2,16384]{2,1,0:T(2,128)(2,1)} async-done(((bf16[8,2,16384]{2,1,0:T(2,128)(2,1)}), bf16[8,2,16384]{2,1,0:T(2,128)(2,1)}, u32[]{:S(2)}, u32[]{:S(2)}) %all-to-all-start.2) | async-done | bytes 524320 | tf_op jit(solution)/shard_map/all_to_all | solution.py:360
  87.0 2.2 reshape.161
  91.8 27.5 %while.10 = (s32[]{:T(128)}, bf16[4,256,2,128]{3,2,1,0:T(2,128)(2,1)S(1)}, bf16[4,256,2,2,64]{1,4,3,2,0:T(8,128)(2,1)S(1)}, bf16[1024,2,2,64]{0,3,2,1:T(8,128)(2...) while((s32[]{:T(128)}, ...), condition=%wide.region_4.5_spmd, body=%wide.region_0.4_spmd.sunk | while | flops 274531840 | bytes 19153508 | solution.py:382
  91.8 3.3 %fusion.65 = (f32[2,2,256]{2,1,0:T(2,128)S(1)}, f32[2,2,256,1024]{3,2,1,0:T(8,128)}) fusion(bf16[1024,2,2,64]{0,3,2,1:T(8,128)(2,1)S(1)} %get-tuple-element.149, bf16[4,256,2,2,64]{1,4,3,2,0:T(8,128)(2,1)S(1)} %get-tuple-element.148, s32[]{:T(128)} %get-tuple-element.138), kind=kOutput, calls=%fused_computation.81.clone.1 | convolution fusion | flops 137364480 | bytes 4853764 | tf_op jit(solution)/shard_map/while/body/eval_jaxpr/sub | solution.py:375
  95.1 2.6 broadcast_divide_fusion.2
  98.7 3.3 %fusion.65 = (f32[2,2,256]{2,1,0:T(2,128)S(1)}, f32[2,2,256,1024]{3,2,1,0:T(8,128)}) fusion(bf16[1024,2,2,64]{0,3,2,1:T(8,128)(2,1)S(1)} %get-tuple-element.149, bf16[4,256,2,2,64]{1,4,3,2,0:T(8,128)(2,1)S(1)} %get-tuple-element.148, s32[]{:T(128)} %get-tuple-element.138), kind=kOutput, calls=%fused_computation.81.clone.1 | convolution fusion | flops 137364480 | bytes 4853764 | tf_op jit(solution)/shard_map/while/body/eval_jaxpr/sub | solution.py:375
  102.0 2.6 broadcast_divide_fusion.2
  105.5 3.3 %fusion.65 = (f32[2,2,256]{2,1,0:T(2,128)S(1)}, f32[2,2,256,1024]{3,2,1,0:T(8,128)}) fusion(bf16[1024,2,2,64]{0,3,2,1:T(8,128)(2,1)S(1)} %get-tuple-element.149, bf16[4,256,2,2,64]{1,4,3,2,0:T(8,128)(2,1)S(1)} %get-tuple-element.148, s32[]{:T(128)} %get-tuple-element.138), kind=kOutput, calls=%fused_computation.81.clone.1 | convolution fusion | flops 137364480 | bytes 4853764 | tf_op jit(solution)/shard_map/while/body/eval_jaxpr/sub | solution.py:375
  108.8 2.6 broadcast_divide_fusion.2
  112.4 3.3 %fusion.65 = (f32[2,2,256]{2,1,0:T(2,128)S(1)}, f32[2,2,256,1024]{3,2,1,0:T(8,128)}) fusion(bf16[1024,2,2,64]{0,3,2,1:T(8,128)(2,1)S(1)} %get-tuple-element.149, bf16[4,256,2,2,64]{1,4,3,2,0:T(8,128)(2,1)S(1)} %get-tuple-element.148, s32[]{:T(128)} %get-tuple-element.138), kind=kOutput, calls=%fused_computation.81.clone.1 | convolution fusion | flops 137364480 | bytes 4853764 | tf_op jit(solution)/shard_map/while/body/eval_jaxpr/sub | solution.py:375
  115.7 2.6 broadcast_divide_fusion.2
  119.5 3.8 %reduce.4 = bf16[1024,256]{1,0:T(8,128)(2,1)S(1)} reduce(bf16[1024,1,256]{2,1,0:T(2,128)(2,1)S(1)} %bitcast.128, bf16[]{:T(256)} %broadcast.186), dimensions={1}, to_apply=%bitcast.92.reduce_sub_computation | reduce | bytes 1048578
  124.2 3.8 %all-to-all-start.3 = ((bf16[8,2,16384]{2,1,0:T(2,128)(2,1)}), bf16[8,2,16384]{2,1,0:T(2,128)(2,1)S(1)}, u32[]{:S(2)}, u32[]{:S(2)}) async-start(bf16[8,2,16384]{2,1,0:T(2,128)(2,1)} %reshape.162), calls=%async_computation.3 | async-start | bytes 1048576 | tf_op jit(solution)/shard_map/all_to_all | solution.py:383
  129.5 12.5 %all-to-all-done.3 = bf16[8,2,16384]{2,1,0:T(2,128)(2,1)S(1)} async-done(((bf16[8,2,16384]{2,1,0:T(2,128)(2,1)}), bf16[8,2,16384]{2,1,0:T(2,128)(2,1)S(1)}, u32[]{:S(2)}, u32[]{:S(2)}) %all-to-all-start.3) | async-done | bytes 524320 | tf_op jit(solution)/shard_map/all_to_all | solution.py:383
  143.0 4.8 %multiply_reduce_fusion.2 = (f32[128]{0:T(128)S(1)}, f32[128,2048]{1,0:T(8,128)S(1)}) fusion(bf16[128,2048]{0,1:T(8,128)(2,1)S(1)} %bitcast.133, bf16[2048,2048]{1,0:T(8,128)(2,1)} %param.22), kind=kOutput, calls=%fused_computation.36 | convolution fusion | flops 1074265984 | bytes 9961984 | tf_op jit(solution)/shard_map/dot_general | solution.py:386
  150.0 115.6 %experts.1 = bf16[128,2048]{1,0:T(8,128)(2,1)} custom-call(bf16[128,2048]{1,0:T(8,128)(2,1)} %fusion.32.rows_ref, bf16[384,128]{1,0:T(8,128)(2,1)} %fusion.35.place_ref, f32[128,384]{1,0:T(8,128)} %select_add_fusion.mix_ref, bf16[128,2048]{1,0:T(8,128)(2,1)} %copy-done, f32[1,2048]{1,0:T(1,128)} %bitcast.139, bf16[2048,1024]{1,0:T(8,128)(2,1)} %bitcast.122, ...), custom_call_target="tpu_custom_call" | custom-call | tf_op jit(solution)/shard_map/experts/pallas_call | solution.py:300
  (95 shorter events, 24.6 us)
Async XLA Ops:
  0.0 22.7 %copy-start.1 = (bf16[1,128,2048]{2,1,0:T(8,128)(2,1)S(1)}, bf16[1,128,2048]{2,1,0:T(8,128)(2,1)}, u32[]{:S(2)}) copy-start(bf16[1,128,2048]{2,1,0:T(8,128)(2,1)} %param.18) | copy-start | bytes 1572868
  2.4 33.5 %copy-start.2 = (bf16[1,128,2048]{2,1,0:T(8,128)(2,1)S(1)}, bf16[1,128,2048]{2,1,0:T(8,128)(2,1)}, u32[]{:S(2)}) copy-start(bf16[1,128,2048]{2,1,0:T(8,128)(2,1)} %param.19) | copy-start | bytes 1572868
  15.4 33.7 %all-to-all-start = ((bf16[8,2,16384]{2,1,0:T(2,128)(2,1)}), bf16[8,2,16384]{2,1,0:T(2,128)(2,1)S(1)}, u32[]{:S(2)}, u32[]{:S(2)}) async-start(bf16[8,2,16384]{2,1,0:T(2,128)(2,1)} %reshape.156), calls=%async_computation | async-start | bytes 1048576 | tf_op jit(solution)/shard_map/all_to_all | solution.py:358
  23.4 31.6 %copy-start.10 = (s32[1,128,2]{1,2,0:T(2,128)S(1)}, s32[1,128,2]{1,2,0:T(2,128)}, u32[]{:S(2)}) copy-start(s32[1,128,2]{1,2,0:T(2,128)} %param.27) | copy-start | bytes 3076
  35.0 38.5 %copy-start.7 = (f32[1,128,2]{1,2,0:T(2,128)S(1)}, f32[1,128,2]{1,2,0:T(2,128)}, u32[]{:S(2)}) copy-start(f32[1,128,2]{1,2,0:T(2,128)} %param.28) | copy-start | bytes 3076
  49.1 20.0 %all-to-all-start.1 = ((bf16[8,2,16384]{2,1,0:T(2,128)(2,1)}), bf16[8,2,16384]{2,1,0:T(2,128)(2,1)S(1)}, u32[]{:S(2)}, u32[]{:S(2)}) async-start(bf16[8,2,16384]{2,1,0:T(2,128)(2,1)} %reshape.158), calls=%async_computation.1 | async-start | bytes 1048576 | tf_op jit(solution)/shard_map/all_to_all | solution.py:359
  69.0 18.0 %all-to-all-start.2 = ((bf16[8,2,16384]{2,1,0:T(2,128)(2,1)}), bf16[8,2,16384]{2,1,0:T(2,128)(2,1)}, u32[]{:S(2)}, u32[]{:S(2)}) async-start(bf16[8,2,16384]{2,1,0:T(2,128)(2,1)} %reshape.160), calls=%async_computation.2 | async-start | bytes 1048576 | tf_op jit(solution)/shard_map/all_to_all | solution.py:360
  89.3 1.9 copy-start.3
  89.4 1.9 copy-start.6
  89.4 1.9 copy-start.11
  90.7 1.0 copy-start.4
  124.2 17.8 %all-to-all-start.3 = ((bf16[8,2,16384]{2,1,0:T(2,128)(2,1)}), bf16[8,2,16384]{2,1,0:T(2,128)(2,1)S(1)}, u32[]{:S(2)}, u32[]{:S(2)}) async-start(bf16[8,2,16384]{2,1,0:T(2,128)(2,1)} %reshape.162), calls=%async_computation.3 | async-start | bytes 1048576 | tf_op jit(solution)/shard_map/all_to_all | solution.py:383
  143.0 4.8 %copy-start.5 = (bf16[1,128,2048]{2,1,0:T(8,128)(2,1)S(1)}, bf16[1,128,2048]{2,1,0:T(8,128)(2,1)}, u32[]{:S(2)}) copy-start(bf16[1,128,2048]{2,1,0:T(8,128)(2,1)} %param.23) | copy-start | bytes 1572868
  143.0 4.8 %copy-start.8 = (f32[2048]{0:T(1024)S(1)}, f32[2048]{0:T(1024)}, u32[]{:S(2)}) copy-start(f32[2048]{0:T(1024)} %param.24) | copy-start | bytes 24580
  143.0 6.0 %copy-start.9 = (f32[2048]{0:T(1024)S(1)}, f32[2048]{0:T(1024)}, u32[]{:S(2)}) copy-start(f32[2048]{0:T(1024)} %param.25) | copy-start | bytes 24580
  148.2 0.8 copy-start

commit v2 on v1

--- a/solution.py
+++ b/solution.py
@@ -9,28 +9,261 @@
 from jax.sharding import PartitionSpec as P
 
 
-def rotate(field):
-    dim_full = field.shape[-1]
-    dim_half = dim_full // 2
-    inverse = 1.0 / 10000.0 ** (jnp.arange(0, dim_full, 2, dtype=jnp.float32) / dim_full)
-    angles = jnp.arange(field.shape[-4], dtype=jnp.float32)[:, None] * inverse[None, :]
-    cosine = jnp.cos(angles)[:, None, None, :]
-    sine_table = jnp.sin(angles)[:, None, None, :]
-    floats = field.astype(jnp.float32)
-    front_part = floats[..., :dim_half]
-    second = floats[..., dim_half:]
-    turned = jnp.concatenate(
-        [front_part * cosine - second * sine_table, second * cosine + front_part * sine_table],
-        axis=-1,
-    )
-    return turned.astype(jnp.bfloat16)
+MESH = pl.DeviceIdType.MESH
 
 
 def rms_scale(values, epsilon):
     return values * lax.rsqrt(jnp.mean(values * values, axis=-1, keepdims=True) + epsilon)
 
 
-MESH = pl.DeviceIdType.MESH
+def attention_kernel(
+    count,
+    heads,
+    query_ref,
+    key_ref,
+    value_ref,
+    cos_ref,
+    sin_ref,
+    lambda_ref,
+    head_gain_ref,
+    residual_ref,
+    mixer_gain_ref,
+    channel_gain_ref,
+    weight_hbm,
+    stream_ref,
+    normed_ref,
+    query_out,
+    key_out,
+    query_in,
+    key_in,
+    value_in,
+    head_out,
+    token_rows,
+    projected,
+    weight,
+    w_sem,
+    in_send,
+    in_recv,
+    out_send,
+    out_recv,
+):
+    me = lax.axis_index("sp")
+    tokens, model = query_ref.shape
+    lanes = head_gain_ref.shape[1]
+    map_dim = lanes // 2
+    scale = map_dim ** (-0.5)
+    load = pltpu.make_async_copy(weight_hbm, weight, w_sem)
+    load.start()
+
+    def sp_at(step):
+        return {"sp": (me + step + count) % count}
+
+    def columns(owner, h):
+        return pl.ds(pl.multiple_of((owner * heads + h) * lanes, lanes), lanes)
+
+    def dest_columns(k, h):
+        return columns((me + k) % count, h)
+
+    def remote(src, dst, send, recv, step):
+        return pltpu.make_async_remote_copy(
+            src_ref=src,
+            dst_ref=dst,
+            send_sem=send,
+            recv_sem=recv,
+            device_id=sp_at(step),
+            device_id_type=MESH,
+        )
+
+    def inward(h, k, i):
+        sources = (value_ref.at[:, dest_columns(k, h)], query_out.at[h, k], key_out.at[h, k])
+        targets = (value_in.at[h, k], query_in.at[h, k], key_in.at[h, k])
+        return remote(sources[i], targets[i], in_send.at[h, i, k], in_recv.at[h, i, k], k)
+
+    def outward(h, k):
+        return remote(
+            head_out.at[h, k], token_rows.at[:, columns(me, h)], out_send.at[h, k], out_recv.at[h, k], -k
+        )
+
+    barrier = pltpu.get_barrier_semaphore()
+    for k in range(1, count):
+        pl.semaphore_signal(barrier, inc=1, device_id=sp_at(k), device_id_type=MESH)
+
+    first_half = lax.broadcasted_iota(jnp.int32, (tokens, lanes), 1) % map_dim < map_dim // 2
+
+    def turned(ref, cols):
+        x = ref[:, cols].astype(jnp.float32)
+        ahead = pltpu.roll(x, lanes - map_dim // 2, 1)
+        behind = pltpu.roll(x, map_dim // 2, 1)
+        return x * cos_ref[...] + jnp.where(first_half, ahead, behind) * sin_ref[...]
+
+    def prepare(h, k):
+        cols = dest_columns(k, h)
+        query = (turned(query_ref, cols) * scale).astype(jnp.bfloat16)
+        key = turned(key_ref, cols).astype(jnp.bfloat16)
+        return query, key
+
+    for h in range(heads):
+        query, key = prepare(h, 0)
+        query_in[h, 0] = query
+        key_in[h, 0] = key
+        value_in[h, 0] = value_ref[:, columns(me, h)]
+
+    pl.semaphore_wait(barrier, count - 1)
+
+    for h in range(heads):
+
+        @pl.loop(1, count)
+        def _(k):
+            inward(h, k, 0).start()
+
+        @pl.loop(1, count)
+        def _(k):
+            query_out[h, k], key_out[h, k] = prepare(h, k)
+
+        @pl.loop(1, count)
+        def _(k):
+            inward(h, k, 1).start()
+            inward(h, k, 2).start()
+
+    width = 2
+    rows = width * tokens
+    length = count * tokens
+    in_first = lax.broadcasted_iota(jnp.int32, (rows, lanes), 1) < map_dim
+
+    def part_of(total):
+        return jnp.exp(total - jnp.max(total, axis=-1, keepdims=True))
+
+    for h in range(heads):
+
+        @pl.loop(1, count)
+        def _(k):
+            for i in range(3):
+                inward(h, k, i).wait_recv()
+
+        @pl.loop(0, count // width)
+        def _(b):
+            query = query_in[h, pl.ds(b * width, width)].reshape(rows, lanes).astype(jnp.float32)
+            both = jnp.concatenate(
+                [jnp.where(in_first, query, 0.0), jnp.where(in_first, 0.0, query)], axis=0
+            ).astype(jnp.bfloat16)
+            keys = key_in[h].reshape(length, lanes)
+            scores = lax.dot_general(
+                both, keys, (((1,), (1,)), ((), ())), preferred_element_type=jnp.float32
+            )
+            one, two = part_of(scores[:rows]), part_of(scores[rows:])
+            one_scale = 1.0 / jnp.sum(one, axis=-1, keepdims=True)
+            two_scale = lambda_ref[h] / jnp.sum(two, axis=-1, keepdims=True)
+            mixing = (one * one_scale - two * two_scale).astype(jnp.bfloat16)
+            mix = jnp.dot(
+                mixing, value_in[h].reshape(length, lanes), preferred_element_type=jnp.float32
+            )
+            result = (rms_scale(mix, 1e-05) * head_gain_ref[...]).astype(jnp.bfloat16)
+            head_out[h, pl.ds(b * width, width)] = result.reshape(width, tokens, lanes)
+            for i in range(width):
+                k = b * width + i
+
+                @pl.when(k > 0)
+                def _():
+                    outward(h, k).start()
+
+    for h in range(heads):
+        token_rows[:, columns(me, h)] = head_out[h, 0]
+
+    load.wait()
+    for h in range(heads):
+
+        @pl.loop(1, count)
+        def _(k):
+            outward(h, k).wait_recv()
+
+    wide = math.gcd(model, 512)
+
+    @pl.loop(0, model // wide)
+    def _(n):
+        cols = pl.ds(pl.multiple_of(n * wide, wide), wide)
+        projected[:, cols] = jnp.dot(
+            token_rows[...], weight[:, cols], preferred_element_type=jnp.float32
+        )
+
+    chunk = math.gcd(tokens, 16)
+
+    @pl.loop(0, tokens // chunk)
+    def _(n):
+        part = pl.ds(pl.multiple_of(n * chunk, chunk), chunk)
+        stream = residual_ref[part, :].astype(jnp.float32)
+        stream = stream + rms_scale(projected[part, :], 1e-06) * mixer_gain_ref[...]
+        stream = stream.astype(jnp.bfloat16)
+        stream_ref[part, :] = stream
+        normed = rms_scale(stream.astype(jnp.float32), 1e-06) * channel_gain_ref[...]
+        normed_ref[part, :] = normed.astype(jnp.bfloat16)
+
+    for h in range(heads):
+
+        @pl.loop(1, count)
+        def _(k):
+            for i in range(3):
+                inward(h, k, i).wait_send()
+            outward(h, k).wait_send()
+
+
+def attention_stage(
+    queries, keys, values, lambdas, head_gain, out_weight, residual, mixer_gain, channel_gain
+):
+    count = lax.axis_size("sp")
+    heads = lambdas.shape[0]
+    lanes = head_gain.shape[0]
+    map_dim = lanes // 2
+    tokens, model = residual.shape
+    inverse = 1.0 / 10000.0 ** (jnp.arange(0, map_dim, 2, dtype=jnp.float32) / map_dim)
+    positions = lax.axis_index("sp") * tokens + jnp.arange(tokens, dtype=jnp.int32)
+    angles = positions.astype(jnp.float32)[:, None] * inverse[None, :]
+    cosine, sine = jnp.cos(angles), jnp.sin(angles)
+    cos_table = jnp.concatenate([cosine] * 4, axis=1)
+    sin_table = jnp.concatenate([-sine, sine] * 2, axis=1)
+    vmem = pl.BlockSpec(memory_space=pltpu.VMEM)
+    smem = pl.BlockSpec(memory_space=pltpu.SMEM)
+    half = jnp.bfloat16
+    dma = pltpu.SemaphoreType.DMA
+    blocks = pltpu.VMEM((heads, count, tokens, lanes), half)
+    shape = jax.ShapeDtypeStruct((tokens, model), half)
+    return pl.pallas_call(
+        functools.partial(attention_kernel, count, heads),
+        out_shape=[shape, shape],
+        in_specs=[vmem] * 5 + [smem] + [vmem] * 4 + [pl.BlockSpec(memory_space=pl.ANY)],
+        out_specs=[vmem, vmem],
+        scratch_shapes=[
+            blocks,
+            blocks,
+            blocks,
+            blocks,
+            blocks,
+            blocks,
+            pltpu.VMEM((tokens, heads * count * lanes), half),
+            pltpu.VMEM((tokens, model), jnp.float32),
+            pltpu.VMEM(out_weight.shape, half),
+            dma,
+            dma((heads, 3, count)),
+            dma((heads, 3, count)),
+            dma((heads, count)),
+            dma((heads, count)),
+        ],
+        compiler_params=pltpu.CompilerParams(
+            collective_id=2, has_side_effects=True, vmem_limit_bytes=60 * 1024 * 1024
+        ),
+        name="attention",
+    )(
+        queries,
+        keys,
+        values,
+        cos_table,
+        sin_table,
+        lambdas,
+        head_gain[None, :],
+        residual,
+        mixer_gain[None, :],
+        channel_gain[None, :],
+        out_weight,
+    )
 
 
 def expert_kernel(
@@ -352,56 +585,28 @@
     up_weight,
     down_weight,
 ):
-    head_count = lambdas.shape[0]
-    head_dim = head_gain.shape[0] // 2
-    seq_query, seq_keys, seq_values = (
-        lax.all_to_all(queries, "sp", split_axis=2, concat_axis=1, tiled=True),
-        lax.all_to_all(key_rows, "sp", split_axis=2, concat_axis=1, tiled=True),
-        lax.all_to_all(value_rows, "sp", split_axis=2, concat_axis=1, tiled=True),
+    stream, normed = attention_stage(
+        queries[0],
+        key_rows[0],
+        value_rows[0],
+        lambdas,
+        head_gain,
+        out_weight,
+        residual[0],
+        mixer_gain,
+        channel_gain,
     )
-    length = seq_query.shape[1]
-    query_rot = rotate(seq_query.reshape(length, head_count, 2, head_dim))
-    keys_rot = rotate(seq_keys.reshape(length, head_count, 2, head_dim))
-    values_heads = seq_values.reshape(length, head_count, 2 * head_dim)
-    block_rows = math.gcd(length, 256)
-    query_blocks = query_rot.reshape(length // block_rows, block_rows, head_count, 2, head_dim)
-    scale = head_dim ** (-0.5)
-
-    def one_block(query_block):
-        scores = (
-            jnp.einsum("qhcd,khcd->hcqk", query_block, keys_rot, preferred_element_type=jnp.float32)
-            * scale
-        )
-        probs = jax.nn.softmax(scores, axis=-1)
-        mixing = (probs[:, 0] - lambdas[:, None, None] * probs[:, 1]).astype(jnp.bfloat16)
-        head_mix = jnp.einsum(
-            "hqk,khv->qhv", mixing, values_heads, preferred_element_type=jnp.float32
-        )
-        return (rms_scale(head_mix, 1e-05) * head_gain).astype(jnp.bfloat16)
-
-    head_out = lax.map(one_block, query_blocks).reshape(1, length, head_count * 2 * head_dim)
-    token_rows = lax.all_to_all(head_out, "sp", split_axis=1, concat_axis=2, tiled=True)
-    tokens = residual.shape[1]
-    model_dim = residual.shape[2]
-    projected = jnp.dot(
-        token_rows.reshape(tokens, -1), out_weight, preferred_element_type=jnp.float32
-    )
-    stream = (
-        residual.reshape(tokens, model_dim).astype(jnp.float32)
-        + rms_scale(projected, 1e-06) * mixer_gain
-    ).astype(jnp.bfloat16)
-    normed = (rms_scale(stream.astype(jnp.float32), 1e-06) * channel_gain).astype(jnp.bfloat16)
     updated = expert_stage(
         normed,
         stream,
-        routes.reshape(tokens, -1),
-        route_logits.reshape(tokens, -1),
+        routes[0],
+        route_logits[0],
         expert_gain,
         gate_weight[0],
         up_weight[0],
         down_weight[0],
     )
-    return updated.reshape(1, tokens, model_dim)
+    return updated[None]
 
 
 def solution(mesh):

time: 268 us -> 186 us (0.69)
  Pallas kernels: 116 us -> 177 us
  other arithmetic: 55.3 us -> 6.12 us
  waiting for transfers between devices: 33.9 us -> 0 us
  starting transfers between devices: 21.4 us -> 0 us
  matrix products: 20.5 us -> 0.2 us
  local copies, waits for them, and re-layouts: 20.2 us -> 2.34 us
    pallas_call x0 -> x1, Pallas kernels: none -> 65.1 us  [attention_stage(): pl.pallas_call(functools.partial(attention_kernel, count, heads), out_sha...]
    unnamed x4 -> x0, other arithmetic: 38.3 us -> none
    all_to_all x4 -> x0, waiting for transfers between devices: 33.9 us -> none  [the longest x1 13.2 us: local(): lax.all_to_all(key_rows, 'sp', split_axis=2, concat_axis=1, tiled=True)]
    all_to_all x4 -> x0, starting transfers between devices: 21.4 us -> none  [the longest x1 7.28 us: local(): lax.all_to_all(queries, 'sp', split_axis=2, concat_axis=1, tiled=True)]
    unnamed x39 -> x1, local copies, waits for them, and re-layouts: 15.3 us -> 1.88 us
    sub x4 -> x0, matrix products: 13.2 us -> none  [one_block(): probs = jax.nn.softmax(scores, axis=-1)]
    div x4 -> x0, other arithmetic: 10.5 us -> none  [one_block(): probs = jax.nn.softmax(scores, axis=-1)]
    dot_general x5 -> x0, matrix products: 7.09 us -> none  [the longest x1 4.79 us: local(): jnp.dot(token_rows.reshape(tokens, -1), out_weight, preferred_element_typ...]
  transfers between devices with their start and end apart: 4 -> 0, of which waited for: 3 -> 0; matrix products, arithmetic and copies ran while one was open for 13% -> 0% of each run, Pallas kernels for 0% -> 0%
where the time goes in v2:
time: 186 us; the launch traced here: 185 us
  Pallas kernels  177 us (95%)
  other arithmetic  6.12 us (3%)
  local copies, waits for them, and re-layouts  2.34 us (1%)
    pallas_call x1, Pallas kernels, expert_stage(): pl.pallas_call(functools.partial(expert_kernel, count, groups), out_shape...  112 us
    pallas_call x1, Pallas kernels, attention_stage(): pl.pallas_call(functools.partial(attention_kernel, count, heads), out_sha...  65.1 us

profile of v2, /device:TPU:0, one launch (start us, length us, event | category | flops | bytes accessed | tf_op | source)
XLA Modules:
  0.0 185.4 jit_solution(10068904347399011463)
XLA Ops:
  0.0 0.7 reduce_max.9
  0.7 0.7 fusion.11
  1.4 0.7 fusion.10
  2.1 0.7 subtract_add_fusion
  2.8 0.1 copy.21
  2.9 0.1 add.63
  3.1 0.2 fusion
  3.3 0.1 sub.31
  3.4 0.1 copy.22
  3.5 0.7 fusion.6
  4.2 0.7 fusion.2.place_ref
  4.9 0.8 select_add_fusion.mix_ref
  5.7 0.3 fusion.3
  6.0 0.8 pad_maximum_fusion
  6.8 65.1 %attention.1 = (bf16[128,2048]{1,0:T(8,128)(2,1)}, bf16[128,2048]{1,0:T(8,128)(2,1)}) custom-call(bf16[128,2048]{1,0:T(8,128)(2,1)} %bitcast.34, bf16[128,2048]{1,0:T(8,128)(2,1)} %bitcast.35, bf16[128,2048]{1,0:T(8,128)(2,1)} %bitcast.36, f32[128,128]{1,0:T(8,128)} %get-tuple-element.16.cos_ref, f32[128,128]{1,0:T(8,128)} %get-tuple-element.17.sin_ref, ...), custom_call_target="tpu_custom_call" | custom-call | tf_op jit(solution)/shard_map/attention/pallas_call | solution.py:229
  71.9 111.6 %experts.1 = bf16[128,2048]{1,0:T(8,128)(2,1)} custom-call(bf16[128,2048]{1,0:T(8,128)(2,1)} %get-tuple-element.7.rows_ref, bf16[384,128]{1,0:T(8,128)(2,1)} %fusion.2.place_ref, f32[128,384]{1,0:T(8,128)} %select_add_fusion.mix_ref, bf16[128,2048]{1,0:T(8,128)(2,1)} %get-tuple-element.8.stream_ref, f32[1,2048]{1,0:T(1,128)} %bitcast.38, ...), custom_call_target="tpu_custom_call" | custom-call | tf_op jit(solution)/shard_map/experts/pallas_call | solution.py:533
  183.5 1.9 %copy.24 = bf16[1,128,2048]{2,1,0:T(8,128)(2,1)} copy(bf16[1,128,2048]{2,1,0:T(8,128)(2,1)} %bitcast.33) | data formatting | bytes 1048576
  (6 shorter events, 0.0 us)

commit v3 on v2

--- a/solution.py
+++ b/solution.py
@@ -29,9 +29,13 @@
     residual_ref,
     mixer_gain_ref,
     channel_gain_ref,
+    routes_ref,
+    logits_ref,
     weight_hbm,
     stream_ref,
     normed_ref,
+    place_ref,
+    mix_ref,
     query_out,
     key_out,
     query_in,
@@ -61,8 +65,11 @@
     def columns(owner, h):
         return pl.ds(pl.multiple_of((owner * heads + h) * lanes, lanes), lanes)
 
+    def far(k):
+        return count // 2 + (k // 2) * (2 * (k % 2) - 1)
+
     def dest_columns(k, h):
-        return columns((me + k) % count, h)
+        return columns((me + far(k)) % count, h)
 
     def remote(src, dst, send, recv, step):
         return pltpu.make_async_remote_copy(
@@ -77,11 +84,11 @@
     def inward(h, k, i):
         sources = (value_ref.at[:, dest_columns(k, h)], query_out.at[h, k], key_out.at[h, k])
         targets = (value_in.at[h, k], query_in.at[h, k], key_in.at[h, k])
-        return remote(sources[i], targets[i], in_send.at[h, i, k], in_recv.at[h, i, k], k)
+        return remote(sources[i], targets[i], in_send.at[h, i, k], in_recv.at[h, i, k], far(k))
 
     def outward(h, k):
         return remote(
-            head_out.at[h, k], token_rows.at[:, columns(me, h)], out_send.at[h, k], out_recv.at[h, k], -k
+            head_out.at[h, k], token_rows.at[:, columns(me, h)], out_send.at[h, k], out_recv.at[h, k], -far(k)
         )
 
     barrier = pltpu.get_barrier_semaphore()
@@ -96,14 +103,13 @@
         behind = pltpu.roll(x, map_dim // 2, 1)
         return x * cos_ref[...] + jnp.where(first_half, ahead, behind) * sin_ref[...]
 
-    def prepare(h, k):
-        cols = dest_columns(k, h)
+    def prepare(h, cols):
         query = (turned(query_ref, cols) * scale).astype(jnp.bfloat16)
         key = turned(key_ref, cols).astype(jnp.bfloat16)
         return query, key
 
     for h in range(heads):
-        query, key = prepare(h, 0)
+        query, key = prepare(h, columns(me, h))
         query_in[h, 0] = query
         key_in[h, 0] = key
         value_in[h, 0] = value_ref[:, columns(me, h)]
@@ -118,12 +124,40 @@
 
         @pl.loop(1, count)
         def _(k):
-            query_out[h, k], key_out[h, k] = prepare(h, k)
+            query_out[h, k], key_out[h, k] = prepare(h, dest_columns(k, h))
 
         @pl.loop(1, count)
         def _(k):
             inward(h, k, 1).start()
             inward(h, k, 2).start()
+
+    top = routes_ref.shape[1]
+    capacity = mix_ref.shape[1] // count
+    experts = lax.broadcasted_iota(jnp.int32, (tokens, 128), 1)
+    places = lax.broadcasted_iota(jnp.int32, mix_ref.shape, 1)
+    lower = lax.broadcasted_iota(jnp.int32, (tokens, tokens), 0)
+    lower = (lower >= lax.broadcasted_iota(jnp.int32, (tokens, tokens), 1)).astype(jnp.bfloat16)
+    logits = logits_ref[...]
+    odds = jnp.exp(logits - jnp.max(logits, axis=-1, keepdims=True))
+    shares = odds / jnp.sum(odds, axis=-1, keepdims=True)
+    used = jnp.zeros((1, 128), jnp.float32)
+    mix = jnp.zeros(mix_ref.shape, jnp.float32)
+    place = jnp.zeros(mix_ref.shape, jnp.float32)
+    for i in range(top):
+        away = routes_ref[:, i : i + 1] - me
+        away = jnp.where(away < 0, away + count, away)
+        mid = count // 2
+        ranked = jnp.where(away < mid, 2 * (mid - away), 2 * (away - mid) + 1)
+        ranked = jnp.where(away == 0, 0, ranked)
+        named = (experts == ranked).astype(jnp.float32)
+        running = jnp.dot(lower, named.astype(jnp.bfloat16), preferred_element_type=jnp.float32)
+        slot = jnp.sum(named * (running + used), axis=-1, keepdims=True).astype(jnp.int32) - 1
+        used = used + jnp.sum(named, axis=0, keepdims=True)
+        hit = places == ranked * capacity + slot
+        mix = mix + jnp.where(hit, shares[:, i : i + 1], 0.0)
+        place = place + jnp.where(hit, 1.0, 0.0)
+    mix_ref[...] = mix
+    place_ref[...] = place.astype(jnp.bfloat16)
 
     width = 2
     rows = width * tokens
@@ -207,7 +241,17 @@
 
 
 def attention_stage(
-    queries, keys, values, lambdas, head_gain, out_weight, residual, mixer_gain, channel_gain
+    queries,
+    keys,
+    values,
+    lambdas,
+    head_gain,
+    out_weight,
+    residual,
+    mixer_gain,
+    channel_gain,
+    routes,
+    logits,
 ):
     count = lax.axis_size("sp")
     heads = lambdas.shape[0]
@@ -226,11 +270,18 @@
     dma = pltpu.SemaphoreType.DMA
     blocks = pltpu.VMEM((heads, count, tokens, lanes), half)
     shape = jax.ShapeDtypeStruct((tokens, model), half)
+    capacity = -(-max(2, 3 * tokens // count) // 16) * 16
+    table = (tokens, count * capacity)
     return pl.pallas_call(
         functools.partial(attention_kernel, count, heads),
-        out_shape=[shape, shape],
-        in_specs=[vmem] * 5 + [smem] + [vmem] * 4 + [pl.BlockSpec(memory_space=pl.ANY)],
-        out_specs=[vmem, vmem],
+        out_shape=[
+            shape,
+            shape,
+            jax.ShapeDtypeStruct(table, half),
+            jax.ShapeDtypeStruct(table, jnp.float32),
+        ],
+        in_specs=[vmem] * 5 + [smem] + [vmem] * 6 + [pl.BlockSpec(memory_space=pl.ANY)],
+        out_specs=[vmem] * 4,
         scratch_shapes=[
             blocks,
             blocks,
@@ -262,6 +313,8 @@
         residual,
         mixer_gain[None, :],
         channel_gain[None, :],
+        routes,
+        logits,
         out_weight,
     )
 
@@ -311,6 +364,9 @@
     def chip_at(step):
         return {"sp": me, "dp": ((chip + step + groups) % groups) * 2 + core}
 
+    def far(k):
+        return count // 2 + (k // 2) * (2 * (k % 2) - 1)
+
     def sp_at(step):
         return {"sp": (me + step + count) % count, "dp": dp}
 
@@ -320,7 +376,7 @@
         )
 
     def send_out(k):
-        return remote(outgoing.at[k], arrived.at[k, 0, 0], a_send.at[k], a_recv.at[k], sp_at(k))
+        return remote(outgoing.at[k], arrived.at[k, 0, 0], a_send.at[k], a_recv.at[k], sp_at(far(k)))
 
     def cross_out(k, j):
         return remote(arrived.at[k, 0, 0], arrived.at[k, 0, j], b_send.at[k, j], b_recv.at[k, j], chip_at(j))
@@ -335,7 +391,7 @@
         return remote(own.at[k, j], cross_in.at[k, j], e_send.at[k, j], e_recv.at[k, j], chip_at(-j))
 
     def send_back(k):
-        return remote(final.at[k], returned.at[k], f_send.at[k], f_recv.at[k], sp_at(-k))
+        return remote(final.at[k], returned.at[k], f_send.at[k], f_recv.at[k], sp_at(-far(k)))
 
     weights = [
         pltpu.make_async_copy(hbm, vmem, w_sem.at[i])
@@ -357,7 +413,9 @@
     @pl.loop(0, model // wide)
     def _(n):
         cols = pl.ds(pl.multiple_of(n * wide, wide), wide)
-        block = jnp.dot(place_ref[...], rows_ref[:, cols], preferred_element_type=jnp.float32)
+        block = lax.dot_general(
+            place_ref[...], rows_ref[:, cols], (((0,), (0,)), ((), ())), preferred_element_type=jnp.float32
+        )
         block = block.astype(jnp.bfloat16).reshape(count, capacity, wide)
         arrived[0, 0, 0, :, cols] = block[0]
         outgoing[:, :, cols] = block
@@ -368,7 +426,7 @@
     def _(k):
         send_out(k).start()
 
-    width = 2
+    width = 1
     rounds = count // width
 
     def per_k(group, action):
@@ -504,29 +562,12 @@
         pair_out(k).wait_send()
 
 
-def expert_stage(normed, stream, routes, logits, expert_gain, gate_weight, up_weight, down_weight):
+def expert_stage(normed, stream, place, mix, expert_gain, gate_weight, up_weight, down_weight):
     count, dp_count = lax.axis_size("sp"), lax.axis_size("dp")
     groups = dp_count // 2
     tokens, model = normed.shape
     units = gate_weight.shape[1]
-    top = routes.shape[1]
-    capacity = -(-max(2, 3 * tokens // count) // 16) * 16
-    relative = (routes - lax.axis_index("sp") + count) % count
-    flat = relative.reshape(-1)
-    one_hot = (flat[:, None] == jnp.arange(count, dtype=jnp.int32)[None, :]).astype(jnp.float32)
-    slots = tokens * top
-    lower = (jnp.arange(slots)[:, None] >= jnp.arange(slots)[None, :]).astype(jnp.float32)
-    running = jnp.dot(lower, one_hot, preferred_element_type=jnp.float32)
-    slot = jnp.sum(one_hot * running, axis=1).astype(jnp.int32) - 1
-    target = (flat * capacity + slot).reshape(tokens, top)
-    shares = jax.nn.softmax(logits, axis=-1)
-    places = jnp.arange(count * capacity, dtype=jnp.int32)
-    mix = jnp.zeros((tokens, count * capacity), jnp.float32)
-    place = jnp.zeros((count * capacity, tokens), jnp.bool_)
-    for i in range(top):
-        mix = mix + jnp.where(target[:, i, None] == places[None, :], shares[:, i, None], 0.0)
-        place = place | (target[None, :, i] == places[:, None])
-    place = place.astype(jnp.bfloat16)
+    capacity = mix.shape[1] // count
     vmem, anywhere = pl.BlockSpec(memory_space=pltpu.VMEM), pl.BlockSpec(memory_space=pl.ANY)
     half = jnp.bfloat16
     dma = pltpu.SemaphoreType.DMA
@@ -543,7 +584,7 @@
             pltpu.VMEM((count, groups, capacity, model), half),
             pltpu.VMEM((count, capacity, model), half),
             pltpu.VMEM((count, capacity, model), half),
-            pltpu.VMEM((4 * groups * capacity, units), half),
+            pltpu.VMEM((2 * groups * capacity, units), half),
             pltpu.VMEM((model, units), half),
             pltpu.VMEM((model, units), half),
             pltpu.VMEM((units, model), half),
@@ -585,7 +626,7 @@
     up_weight,
     down_weight,
 ):
-    stream, normed = attention_stage(
+    stream, normed, place, mix = attention_stage(
         queries[0],
         key_rows[0],
         value_rows[0],
@@ -595,12 +636,14 @@
         residual[0],
         mixer_gain,
         channel_gain,
+        routes[0],
+        route_logits[0],
     )
     updated = expert_stage(
         normed,
         stream,
-        routes[0],
-        route_logits[0],
+        place,
+        mix,
         expert_gain,
         gate_weight[0],
         up_weight[0],

time: 186 us -> 171 us (0.919)
  Pallas kernels: 177 us -> 165 us
  other arithmetic: 6.12 us -> 1.14 us
  local copies, waits for them, and re-layouts: 2.34 us -> 4.71 us
    pallas_call x1, Pallas kernels: 112 us -> 104 us  [expert_stage(): pl.pallas_call(functools.partial(expert_kernel, count, groups), out_shape...]
    pallas_call x1, Pallas kernels: 65.1 us -> 60.5 us  [attention_stage(): pl.pallas_call(functools.partial(attention_kernel, count, heads), out_sha...]
    unnamed x1 -> x3, local copies, waits for them, and re-layouts: 1.88 us -> 4.71 us
    add x3 -> x0, other arithmetic: 2.22 us -> none  [the longest x1 0.81 us: expert_stage(): mix + jnp.where(target[:, i, None] == places[None, :], shares[:, i, None]...]
where the time goes in v3:
time: 171 us
  Pallas kernels  165 us (96%)
  local copies, waits for them, and re-layouts  4.71 us (3%)
    pallas_call x1, Pallas kernels, expert_stage(): pl.pallas_call(functools.partial(expert_kernel, count, groups), out_shape...  104 us
    pallas_call x1, Pallas kernels, attention_stage(): pl.pallas_call(functools.partial(attention_kernel, count, heads), out_sha...  60.5 us
    unnamed x3, local copies, waits for them, and re-layouts  4.71 us

profile of v3, /device:TPU:0, one launch (start us, length us, event | category | flops | bytes accessed | tf_op | source)
XLA Modules:
  0.0 170.7 jit_solution(5632912730630555444)
XLA Ops:
  0.0 1.4 copy.19
  1.4 1.4 copy.20
  2.8 0.3 fusion
  3.2 0.8 pad_maximum_fusion
  4.0 60.5 %attention.1 = (bf16[128,2048]{1,0:T(8,128)(2,1)}, bf16[128,2048]{1,0:T(8,128)(2,1)}, bf16[128,384]{1,0:T(8,128)(2,1)}, f32[128,384]{1,0:T(8,128)}) custom-call(bf16[128,2048]{1,0:T(8,128)(2,1)} %bitcast.18, bf16[128,2048]{1,0:T(8,128)(2,1)} %bitcast.19, bf16[128,2048]{1,0:T(8,128)(2,1)} %bitcast.20, f32[128,128]{1,0:T(8,128)} %get-tuple-element.16.cos_ref, ...), custom_call_target="tpu_custom_call" | custom-call | tf_op jit(solution)/shard_map/attention/pallas_call | solution.py:275
  64.5 104.3 %experts.1 = bf16[128,2048]{1,0:T(8,128)(2,1)} custom-call(bf16[128,2048]{1,0:T(8,128)(2,1)} %get-tuple-element.9.rows_ref, bf16[128,384]{1,0:T(8,128)(2,1)} %get-tuple-element.10.place_ref, f32[128,384]{1,0:T(8,128)} %get-tuple-element.11.mix_ref, bf16[128,2048]{1,0:T(8,128)(2,1)} %get-tuple-element.12.stream_ref, f32[1,2048]{1,0:T(1,128)} %bitcast.24, ...), custom_call_target="tpu_custom_call" | custom-call | tf_op jit(solution)/shard_map/experts/pallas_call | solution.py:574
  168.8 1.9 %copy.22 = bf16[1,128,2048]{2,1,0:T(8,128)(2,1)} copy(bf16[1,128,2048]{2,1,0:T(8,128)(2,1)} %bitcast.17) | data formatting | bytes 1048576
  (2 shorter events, 0.0 us)
